TPU v7x, 32 devices: a whole 2x2x4 slice. The times are simulated.
32 devices in a mesh: grp: 2 (over x), ep: 16 (over z, y, core).
Axes of the slice: x: 2, y: 2, z: 4, core: 2. Of those that a mesh axis runs over, the one named last changes fastest.
Arguments:
- tokens: bfloat16 [512, 2048], P(('grp', 'ep')), parts along dimension 0, may hold values from -6 to 6
- attn_gain: float32 [2048], replicated, may hold values from 0.1 to 1.9
- w_query: bfloat16 [2048, 1024], replicated, may hold values from -0.125 to 0.125
- w_key: bfloat16 [2048, 128], replicated, may hold values from -0.125 to 0.125
- w_value: bfloat16 [2048, 128], replicated, may hold values from -0.125 to 0.125
- w_forget: bfloat16 [2048, 2], replicated, may hold values from -0.125 to 0.125
- forget_bias: float32 [2], replicated, may hold values from -3 to 1
- w_attn_out: bfloat16 [1024, 2048], replicated, may hold values from -0.1875 to 0.1875
- cache_keys: bfloat16 [512, 1024, 128], P(('grp', 'ep')), parts along dimension 0, may hold values from -640 to 640
- cache_values: bfloat16 [512, 1024, 128], P(('grp', 'ep')), parts along dimension 0, may hold values from -6 to 6
- cache_logsum: float32 [512, 2, 1024], P(('grp', 'ep')), parts along dimension 0, may hold values from -100 to 0, as said below
- lengths: int32 [512], P(('grp', 'ep')), parts along dimension 0, may hold values from 1 to 1024, as said below
- ffn_gain: float32 [2048], replicated, may hold values from 0.1 to 1.9
- branch_gate: float32 [2048], replicated, may hold values from -0.125 to 0.125
- dense_gate: bfloat16 [2048, 4096], P(None, 'ep'), may hold values from -0.125 to 0.125
- dense_up: bfloat16 [2048, 4096], P(None, 'ep'), may hold values from -0.125 to 0.125
- dense_down: bfloat16 [4096, 2048], P('ep'), may hold values from -0.09375 to 0.09375
- expert_gate: bfloat16 [16, 2048, 512], P('ep'), may hold values from -0.125 to 0.125
- expert_up: bfloat16 [16, 2048, 512], P('ep'), may hold values from -0.125 to 0.125
- expert_down: bfloat16 [16, 512, 2048], P('ep'), may hold values from -0.25 to 0.25
- routes: int32 [512, 4], P(('grp', 'ep')), parts along dimension 0, may hold values from 0 to 15, all different within a row; in each aligned block of 16 rows (0 to 15, 16 to 31, ...) at most 8 rows name the same one
- route_weights: float32 [512, 4], P(('grp', 'ep')), parts along dimension 0, may hold values from 0.2 to 1
Outputs:
- output_rows: bfloat16 [512, 2048], P(('grp', 'ep')), parts along dimension 0
There are 2 independent parts, one for each index of `grp`. A program takes and returns all parts, laid end to end along the dimension named above; an argument that names none is the same for every part. Nothing has to cross between parts.
Inputs may be any that keep to these rules, and one draw needn't show every extreme that they name: `lengths`: each aligned block of 16 sequences holds one with 1024 valid positions; every length is at least 128. `routes`: a row's 4 experts differ; among the rows of one device no expert is named more than 8 times. `cache_logsum`: non-increasing along positions.
All inputs are finite; a program needn't handle non-finite values.
Results may differ from a plain program's by a relative error of at most 0.012.
The roundings to bfloat16 on the way count: a program that leaves them out, or rounds other values in their place, can miss the bound.
Values may be sent and summed in bfloat16 or wider, within the bound.
No kernel may reach another device: no remote copies, remote signals or barrier semaphores. Data moves between devices by JAX's collectives and lax.ppermute only.
A program may use at most 128 MiB of HBM per device.

v0:
```python
import math
import jax
import jax.numpy as jnp
from jax import lax
from jax.sharding import PartitionSpec as P

EPSILON = 1e-06


def norm_rows(inputs, gain_vec):
    widened = inputs.astype(jnp.float32)
    scaled = widened * lax.rsqrt(jnp.mean(widened * widened, axis=-1, keepdims=True) + EPSILON)
    return (scaled * gain_vec).astype(jnp.bfloat16)


def swiglu(row_block, w_first, w_second):
    gate_part = jnp.dot(row_block, w_first, preferred_element_type=jnp.float32)
    up_part = jnp.dot(row_block, w_second, preferred_element_type=jnp.float32)
    return (jax.nn.silu(gate_part) * up_part).astype(jnp.bfloat16)


def expert_rows(row_block, w_gate, w_up, w_down):
    middle = swiglu(row_block, w_gate, w_up)
    return jnp.dot(middle, w_down, preferred_element_type=jnp.float32).astype(jnp.bfloat16)


def attend(
    normed,
    w_query,
    w_key,
    w_value,
    w_forget,
    forget_bias,
    cache_keys,
    cache_values,
    cache_logsum,
    lengths,
):
    own_rows = normed.shape[0]
    kv_heads = cache_logsum.shape[1]
    cache_span = cache_logsum.shape[2]
    head_size = w_key.shape[1] // kv_heads
    group_size = w_query.shape[1] // head_size // kv_heads
    scaling = 1.0 / math.sqrt(head_size)
    queries = jnp.dot(normed, w_query, preferred_element_type=jnp.float32).astype(jnp.bfloat16)
    new_keys = jnp.dot(normed, w_key, preferred_element_type=jnp.float32).astype(jnp.bfloat16)
    new_values = jnp.dot(normed, w_value, preferred_element_type=jnp.float32).astype(jnp.bfloat16)
    log_gate = jax.nn.log_sigmoid(
        jnp.dot(normed, w_forget, preferred_element_type=jnp.float32) + forget_bias
    )
    positions = lax.broadcasted_iota(jnp.int32, (own_rows, kv_heads, cache_span), 2)
    latest = jnp.sum(jnp.where(positions == lengths[:, None, None] - 1, cache_logsum, 0.0), axis=2)
    offsets = (latest + log_gate)[:, :, None] - cache_logsum
    usable = positions < lengths[:, None, None]
    query_heads = queries.reshape(own_rows, kv_heads, group_size, head_size)
    key_heads = cache_keys.reshape(own_rows, cache_span, kv_heads, head_size)
    value_heads = cache_values.reshape(own_rows, cache_span, kv_heads, head_size)
    scores = (
        jnp.einsum("bgrd,blgd->bgrl", query_heads, key_heads, preferred_element_type=jnp.float32)
        * scaling
    )
    scores = jnp.where(usable[:, :, None, :], scores + offsets[:, :, None, :], -jnp.inf)
    self_score = (
        jnp.einsum(
            "bgrd,bgd->bgr",
            query_heads,
            new_keys.reshape(own_rows, kv_heads, head_size),
            preferred_element_type=jnp.float32,
        )
        * scaling
    )
    peak_score = jnp.maximum(jnp.max(scores, axis=3), self_score)
    cache_weight = jnp.exp(scores - peak_score[..., None])
    self_weight = jnp.exp(self_score - peak_score)
    denominator = jnp.sum(cache_weight, axis=3) + self_weight
    cache_probs = (cache_weight / denominator[..., None]).astype(jnp.bfloat16)
    self_probs = (self_weight / denominator).astype(jnp.bfloat16)
    attended = jnp.einsum(
        "bgrl,blgd->bgrd", cache_probs, value_heads, preferred_element_type=jnp.float32
    )
    attended = attended + self_probs.astype(jnp.float32)[..., None] * new_values.reshape(
        own_rows, kv_heads, 1, head_size
    ).astype(jnp.float32)
    return attended.reshape(own_rows, -1).astype(jnp.bfloat16)


def body(
    tokens,
    attn_gain,
    w_query,
    w_key,
    w_value,
    w_forget,
    forget_bias,
    w_attn_out,
    cache_keys,
    cache_values,
    cache_logsum,
    lengths,
    ffn_gain,
    branch_gate,
    dense_gate,
    dense_up,
    dense_down,
    expert_gate,
    expert_up,
    expert_down,
    routes,
    route_weights,
):
    own_rows = tokens.shape[0]
    normed = norm_rows(tokens, attn_gain)
    attended = attend(
        normed,
        w_query,
        w_key,
        w_value,
        w_forget,
        forget_bias,
        cache_keys,
        cache_values,
        cache_logsum,
        lengths,
    )
    residual = tokens.astype(jnp.float32) + jnp.dot(
        attended, w_attn_out, preferred_element_type=jnp.float32
    )
    second = norm_rows(residual, ffn_gain)
    branch_share = jax.nn.sigmoid(
        jnp.dot(second.astype(jnp.float32), branch_gate, precision=lax.Precision.HIGHEST)
    )
    expert_count = lax.axis_size("ep")
    route_count = routes.shape[1]
    capacity = max(2, 2 * own_rows * route_count // expert_count)
    hits = (
        routes[:, :, None]
        == lax.broadcasted_iota(jnp.int32, (own_rows, route_count, expert_count), 2)
    ).astype(jnp.int32)
    flat_hits = hits.reshape(own_rows * route_count, expert_count)
    order_rank = jnp.sum((jnp.cumsum(flat_hits, axis=0) - 1) * flat_hits, axis=1).reshape(
        own_rows, route_count
    )
    slot_index = routes * capacity + order_rank
    slot_total = expert_count * capacity
    matches = slot_index[None, :, :] == lax.broadcasted_iota(
        jnp.int32, (slot_total, own_rows, route_count), 0
    )
    dispatch = jnp.sum(matches.astype(jnp.float32), axis=2).astype(jnp.bfloat16)
    combine = jnp.sum(jnp.where(matches, route_weights[None, :, :], 0.0), axis=2).T
    outgoing = jnp.dot(dispatch, second, preferred_element_type=jnp.float32).astype(jnp.bfloat16)
    outgoing = outgoing.reshape(expert_count, 1, capacity, -1)
    arrived = lax.all_to_all(outgoing, "ep", split_axis=0, concat_axis=1, tiled=True)
    arrived_shape = arrived.shape
    answer = expert_rows(
        arrived.reshape(-1, arrived_shape[3]), expert_gate[0], expert_up[0], expert_down[0]
    )
    returned = lax.all_to_all(
        answer.reshape(arrived_shape), "ep", split_axis=1, concat_axis=0, tiled=True
    )
    routed = jnp.dot(
        combine,
        returned.reshape(slot_total, -1).astype(jnp.float32),
        precision=lax.Precision.HIGHEST,
    )
    dense_hidden = swiglu(lax.all_gather(second, "ep", axis=0, tiled=True), dense_gate, dense_up)
    dense = lax.psum_scatter(
        jnp.dot(dense_hidden, dense_down, preferred_element_type=jnp.float32).astype(jnp.bfloat16),
        "ep",
        scatter_dimension=0,
        tiled=True,
    ).astype(jnp.float32)
    output_rows = residual + branch_share[:, None] * dense + routed
    return output_rows.astype(jnp.bfloat16)


def solution(mesh):
    return jax.shard_map(
        body,
        mesh=mesh,
        in_specs=(
            P(("grp", "ep"), None),
            P(),
            P(),
            P(),
            P(),
            P(),
            P(),
            P(),
            P(("grp", "ep"), None, None),
            P(("grp", "ep"), None, None),
            P(("grp", "ep"), None, None),
            P(("grp", "ep")),
            P(),
            P(),
            P(None, "ep"),
            P(None, "ep"),
            P("ep", None),
            P("ep", None, None),
            P("ep", None, None),
            P("ep", None, None),
            P(("grp", "ep"), None),
            P(("grp", "ep"), None),
        ),
        out_specs=P(("grp", "ep"), None),
        check_vma=False,
    )
```

profile of v0, /device:TPU:0, one launch (start us, length us, event | category | flops | bytes accessed | tf_op | source)
XLA Modules:
  0.0 152.9 jit_solution(14952245672474803569)
XLA Ops:
  6.5 0.0 copy-start
  6.5 0.0 copy-start.11
  6.6 0.0 all-gather.2.cloned.1.call-start
  6.6 0.8 broadcast_add_fusion
  7.4 0.8 iota_compare_fusion
  8.2 1.0 fusion.43
  9.2 2.9 %convolution_convert_fusion.3 = bf16[16,1024]{1,0:T(8,128)(2,1)S(1)} fusion(bf16[2048,1024]{1,0:T(8,128)(2,1)} %param.24, bf16[16,2048]{1,0:T(8,128)(2,1)} %param.22, f32[2048]{0:T(1024)} %param.23, f32[16]{0:T(128)S(1)} %add_rsqrt_fusion.1), kind=kOutput, calls=%fused_computation.22 | convolution fusion | flops 67256320 | bytes 4300864 | tf_op jit(solution)/shard_map/dot_general | solution.py:45
  12.1 0.1 reshape.95
  12.3 0.0 copy-done.4
  12.3 0.2 fusion.46
  12.5 0.1 copy.54
  12.6 0.0 copy-done.1
  12.6 0.0 copy-done.5
  12.6 0.0 copy-done.9
  12.6 0.0 copy-done.11
  12.6 0.2 fusion.53
  12.8 0.1 copy.55
  12.9 0.1 broadcast_subtract_fusion
  13.0 0.0 copy-start.3
  13.0 6.5 %copy.53 = bf16[16,1024,128]{1,2,0:T(8,128)(2,1)} copy(bf16[16,1024,128]{2,1,0:T(8,128)(2,1)} %param.30) | data formatting | bytes 8388608 | tf_op args[8]
  19.5 0.0 copy-done.3
  19.5 0.2 convolution_convert_fusion.5
  19.7 0.1 reshape.109
  19.8 0.2 fusion.62
  20.0 3.0 %fusion.61 = (f32[16,2,8]{2,1,0:T(2,128)S(1)}, f32[16,2,8,1024]{3,2,1,0:T(8,128)S(1)}) fusion(f32[16,2,1024]{2,1,0:T(2,128)S(1)} %broadcast_subtract_fusion, bf16[16,2,8,64]{3,2,1,0:T(8,128)(2,1)S(1)} %reshape.95, bf16[16,1024,2,64]{1,3,2,0:T(8,128)(2,1)} %bitcast.70, pred[16,2,1024]{2,1,0:T(4,128)(4,1)S(1)} %iota_compare_fusion), kind=kOutput, calls=%fused_computation.85 | convolution fusion | flops 34602752 | bytes 5440512 | tf_op jit(solution)/shard_map/bgrd,blgd->bgrl/dot_general | solution.py:59
  23.0 0.3 fusion.24
  23.3 1.3 fusion.18
  24.6 0.1 reshape.103
  24.7 6.4 %copy.56 = bf16[16,1024,128]{1,2,0:T(8,128)(2,1)} copy(bf16[16,1024,128]{2,1,0:T(8,128)(2,1)} %param.31) | data formatting | bytes 8388608 | tf_op args[9]
  31.1 3.4 %fusion.17 = bf16[16,2,8,64]{3,2,1,0:T(8,128)(2,1)S(1)} fusion(bf16[16,1024,2,64]{1,3,2,0:T(8,128)(2,1)} %bitcast.71, f32[16,2,8,1024]{3,2,1,0:T(8,128)S(1)} %get-tuple-element.10, f32[16,2,8]{2,1,0:T(2,128)S(1)} %get-tuple-element.8, f32[16,2,8]{2,1,0:T(2,128)S(1)} %multiply_maximum_fusion, f32[16,2,64]{2,1,0:T(2,128)S(1)} %reshape.103, ...), kind=kOutput, calls=%fused_computation.21 | convolution fusion | flops 34390016 | bytes 5286912 | tf_op jit(solution)/shard_map/bgrl,blgd->bgrd/dot_general | solution.py:78
  34.5 0.1 convert_element_type.90
  34.7 3.0 %multiply_reduce_fusion = (f32[16]{0:T(128)S(1)}, f32[16,2048]{1,0:T(8,128)S(1)}) fusion(bf16[16,1024]{1,0:T(8,128)(2,1)S(1)} %convert_element_type.90, bf16[1024,2048]{1,0:T(8,128)(2,1)} %param.29, bf16[16,2048]{1,0:T(8,128)(2,1)S(1)} %copy-done.1), kind=kOutput, calls=%fused_computation.61 | convolution fusion | flops 67239920 | bytes 4423744 | tf_op jit(solution)/shard_map/dot_general | solution.py:125
  37.6 0.0 copy-done.6
  37.7 0.7 multiply_convert_fusion
  38.4 0.0 all-gather.2.cloned.1.call-update
  38.4 0.0 copy-done.7
  38.4 0.1 copy.57
  38.5 0.1 eq.31
  38.6 0.1 fusion.49
  38.7 0.1 reduce_window_sum.11
  38.8 0.2 select_reduce_fusion.1
  38.9 0.1 reduce_sum.70
  39.0 0.1 copy.58
  39.1 0.0 copy-done.8
  39.1 0.1 convert_reduce_fusion
  39.2 2.0 %fusion = bf16[16,1,8,2048]{3,2,1,0:T(8,128)(2,1)} fusion(bf16[16,2048]{1,0:T(8,128)(2,1)} %multiply_convert_fusion, bf16[128,16]{0,1:T(8,128)(2,1)S(1)} %get-tuple-element.5), kind=kOutput, calls=%fused_computation.3 | convolution fusion | flops 8650752 | bytes 593920 | tf_op jit(solution)/shard_map/dot_general | solution.py:150
  41.2 7.4 %all-to-all-start = ((bf16[16,1,8,2048]{3,2,1,0:T(8,128)(2,1)}), bf16[16,1,8,2048]{3,2,1,0:T(8,128)(2,1)S(1)}, u32[]{:S(2)}, u32[]{:S(2)}) async-start(bf16[16,1,8,2048]{3,2,1,0:T(8,128)(2,1)} %fusion), calls=%async_computation.1 | async-start | bytes 1048576 | tf_op jit(solution)/shard_map/all_to_all | solution.py:152
  48.6 0.0 reduce-scatter.2.cloned.1.call-start
  48.6 32.8 %all-gather.2.cloned.1.call-done = bf16[256,2048]{1,0:T(8,128)(2,1)} async-done(((bf16[16,2048]{1,0:T(8,128)(2,1)}), bf16[256,2048]{1,0:T(8,128)(2,1)}) %all-gather.2.cloned.1.call-update) | async-done | bytes 1048592 | tf_op jit(solution)/shard_map/all_gather | solution.py:165
  81.5 2.0 %fusion.63 = f32[256,256]{1,0:T(8,128)S(1)} fusion(bf16[256,2048]{1,0:T(8,128)(2,1)} %all-gather.2.cloned.1.call-done, bf16[2048,256]{1,0:T(8,128)(2,1)} %param.36), kind=kOutput, calls=%fused_computation.87 | convolution fusion | flops 268435456 | bytes 2359296 | tf_op jit(solution)/shard_map/dot_general | solution.py:17
  83.4 4.1 %convolution_convert_fusion = bf16[256,2048]{1,0:T(8,128)(2,1)} fusion(bf16[256,2048]{1,0:T(8,128)(2,1)} %param.38, bf16[256,2048]{1,0:T(8,128)(2,1)} %all-gather.2.cloned.1.call-done, bf16[2048,256]{1,0:T(8,128)(2,1)} %param.37, f32[256,256]{1,0:T(8,128)S(1)} %fusion.63), kind=kOutput, calls=%fused_computation | convolution fusion | flops 537788416 | bytes 4456448 | tf_op jit(solution)/shard_map/dot_general | solution.py:167
  87.6 0.0 reduce-scatter.2.cloned.1.call-update
  87.6 0.0 copy-start.2
  87.6 0.0 copy-start.10
  87.6 0.0 all-to-all-done
  87.6 2.0 %fusion.6 = f32[128,512]{1,0:T(8,128)S(1)} fusion(bf16[1,2048,512]{2,1,0:T(8,128)(2,1)} %param.39, bf16[16,1,8,2048]{3,2,1,0:T(8,128)(2,1)S(1)} %all-to-all-done), kind=kOutput, calls=%fused_computation.11 | convolution fusion | flops 268435456 | bytes 2883584 | tf_op jit(solution)/shard_map/dot_general | solution.py:17
  89.7 0.0 copy-done
  89.7 3.2 %fusion.1 = bf16[1,16,8,2048]{3,2,0,1:T(8,128)(2,1)} fusion(bf16[1,512,2048]{2,1,0:T(8,128)(2,1)S(1)} %copy-done, bf16[1,2048,512]{2,1,0:T(8,128)(2,1)} %param.40, bf16[16,1,8,2048]{3,2,1,0:T(8,128)(2,1)S(1)} %all-to-all-done, f32[128,512]{1,0:T(8,128)S(1)} %fusion.6), kind=kOutput, calls=%fused_computation.4 | convolution fusion | flops 537526272 | bytes 5505024 | tf_op jit(solution)/shard_map/dot_general | solution.py:24
  92.9 3.7 %all-to-all-start.1 = ((bf16[1,16,8,2048]{3,2,0,1:T(8,128)(2,1)}), bf16[1,16,8,2048]{3,2,0,1:T(8,128)(2,1)S(1)}, u32[]{:S(2)}, u32[]{:S(2)}) async-start(bf16[1,16,8,2048]{3,2,0,1:T(8,128)(2,1)} %fusion.1), calls=%async_computation.2 | async-start | bytes 1048576 | tf_op jit(solution)/shard_map/all_to_all | solution.py:157
  96.6 0.0 copy-done.2
  96.7 0.1 fusion.23
  96.8 14.1 %all-to-all-done.1 = bf16[1,16,8,2048]{3,2,0,1:T(8,128)(2,1)S(1)} async-done(((bf16[1,16,8,2048]{3,2,0,1:T(8,128)(2,1)}), bf16[1,16,8,2048]{3,2,0,1:T(8,128)(2,1)S(1)}, u32[]{:S(2)}, u32[]{:S(2)}) %all-to-all-start.1) | async-done | bytes 524320 | tf_op jit(solution)/shard_map/all_to_all | solution.py:157
  110.9 33.4 %reduce-scatter.2.cloned.1.call-done = bf16[16,2048]{1,0:T(8,128)(2,1)} async-done(((bf16[256,2048]{1,0:T(8,128)(2,1)}), bf16[16,2048]{1,0:T(8,128)(2,1)}) %reduce-scatter.2.cloned.1.call-update) | async-done | bytes 65552 | tf_op jit(solution)/shard_map/reduce_scatter | solution.py:166
  144.3 1.8 %fusion.2 = bf16[16,2048]{1,0:T(8,128)(2,1)} fusion(f32[128,16]{0,1:T(8,128)S(1)} %get-tuple-element.6, bf16[1,16,8,2048]{3,2,0,1:T(8,128)(2,1)S(1)} %all-to-all-done.1, f32[16,2048]{1,0:T(8,128)S(1)} %get-tuple-element.12, bf16[16,2048]{1,0:T(8,128)(2,1)} %reduce-scatter.2.cloned.1.call-done, f32[16]{0:T(128)S(1)} %fusion.23), kind=kOutput, calls=%fused_computation.7 | convolution fusion | flops 50495488 | bytes 794688 | tf_op jit(solution)/shard_map/dot_general | solution.py:160
  (13 shorter events, 0.1 us)
Async XLA Ops:
  6.5 83.2 %copy-start = (bf16[1,512,2048]{2,1,0:T(8,128)(2,1)S(1)}, bf16[1,512,2048]{2,1,0:T(8,128)(2,1)}, u32[]{:S(2)}) copy-start(bf16[1,512,2048]{2,1,0:T(8,128)(2,1)} %param.41) | copy-start | bytes 6291460
  6.5 6.0 %copy-start.1 = (bf16[16,2048]{1,0:T(8,128)(2,1)S(1)}, bf16[16,2048]{1,0:T(8,128)(2,1)}, u32[]{:S(2)}) copy-start(bf16[16,2048]{1,0:T(8,128)(2,1)} %param.22) | copy-start | bytes 196612
  6.5 6.0 %copy-start.5 = (f32[2048]{0:T(1024)S(1)}, f32[2048]{0:T(1024)}, u32[]{:S(2)}) copy-start(f32[2048]{0:T(1024)} %param.23) | copy-start | bytes 24580
  6.5 5.7 %copy-start.4 = (f32[16,2,1024]{2,1,0:T(2,128)S(1)}, f32[16,2,1024]{2,1,0:T(2,128)}, u32[]{:S(2)}) copy-start(f32[16,2,1024]{2,1,0:T(2,128)} %param.32) | copy-start | bytes 393220
  6.5 6.0 %copy-start.9 = (bf16[2048,2]{0,1:T(2,128)(2,1)S(1)}, bf16[2048,2]{0,1:T(2,128)(2,1)}, u32[]{:S(2)}) copy-start(bf16[2048,2]{0,1:T(2,128)(2,1)} %param.27) | copy-start | bytes 24580
  6.5 6.0 %copy-start.11 = (f32[2]{0:T(128)S(1)}, f32[2]{0:T(128)}, u32[]{:S(2)}) copy-start(f32[2]{0:T(128)} %param.28) | copy-start | bytes 28
  6.6 74.9 %all-gather.2.cloned.1.call-start = ((), (), s32[]{:S(2)}) async-start(), calls=%async_computation.3 | async-start | bytes 1114112 | tf_op jit(solution)/shard_map/all_gather | solution.py:165
  13.0 6.5 %copy-start.3 = (bf16[2048,128]{1,0:T(8,128)(2,1)S(1)}, bf16[2048,128]{1,0:T(8,128)(2,1)}, u32[]{:S(2)}) copy-start(bf16[2048,128]{1,0:T(8,128)(2,1)} %param.25) | copy-start | bytes 1572868
  31.1 6.6 %copy-start.6 = (f32[2048]{0:T(1024)S(1)}, f32[2048]{0:T(1024)}, u32[]{:S(2)}) copy-start(f32[2048]{0:T(1024)} %param.34) | copy-start | bytes 24580
  34.5 3.9 %copy-start.7 = (s32[16,4]{0,1:T(4,128)S(1)}, s32[16,4]{0,1:T(4,128)}, u32[]{:S(2)}) copy-start(s32[16,4]{0,1:T(4,128)} %param.42) | copy-start | bytes 772
  34.5 4.6 %copy-start.8 = (f32[16,4]{0,1:T(4,128)S(1)}, f32[16,4]{0,1:T(4,128)}, u32[]{:S(2)}) copy-start(f32[16,4]{0,1:T(4,128)} %param.43) | copy-start | bytes 772
  41.2 46.4 %all-to-all-start = ((bf16[16,1,8,2048]{3,2,1,0:T(8,128)(2,1)}), bf16[16,1,8,2048]{3,2,1,0:T(8,128)(2,1)S(1)}, u32[]{:S(2)}, u32[]{:S(2)}) async-start(bf16[16,1,8,2048]{3,2,1,0:T(8,128)(2,1)} %fusion), calls=%async_computation.1 | async-start | bytes 1048576 | tf_op jit(solution)/shard_map/all_to_all | solution.py:152
  48.6 95.7 %reduce-scatter.2.cloned.1.call-start = ((), (), s32[]{:S(2)}) async-start(), calls=%async_computation.4 | async-start | bytes 1114112 | tf_op jit(solution)/shard_map/reduce_scatter | solution.py:166
  87.6 9.0 %copy-start.2 = (bf16[16,2048]{1,0:T(8,128)(2,1)S(1)}, bf16[16,2048]{1,0:T(8,128)(2,1)}, u32[]{:S(2)}) copy-start(bf16[16,2048]{1,0:T(8,128)(2,1)} %multiply_convert_fusion) | copy-start | bytes 196612
  87.6 9.0 %copy-start.10 = (f32[2048]{0:T(1024)S(1)}, f32[2048]{0:T(1024)}, u32[]{:S(2)}) copy-start(f32[2048]{0:T(1024)} %param.35) | copy-start | bytes 24580
  92.9 18.0 %all-to-all-start.1 = ((bf16[1,16,8,2048]{3,2,0,1:T(8,128)(2,1)}), bf16[1,16,8,2048]{3,2,0,1:T(8,128)(2,1)S(1)}, u32[]{:S(2)}, u32[]{:S(2)}) async-start(bf16[1,16,8,2048]{3,2,0,1:T(8,128)(2,1)} %fusion.1), calls=%async_computation.2 | async-start | bytes 1048576 | tf_op jit(solution)/shard_map/all_to_all | solution.py:157
Sparse Core Ops, SparseCore 0:
  38.5 42.8 all-gather.1
  87.7 56.5 reduce-scatter.1
where the time goes:
time: 154 us; the launch traced here: 153 us
  waiting for transfers between devices  80.4 us (52%)
  matrix products  29.5 us (19%)
  local copies, waits for them, and re-layouts  13.8 us (9%)
  between operations  13.6 us (9%)
  starting transfers between devices  11.2 us (7%)
  other arithmetic  4.46 us (3%)
    reduce_scatter x1, waiting for transfers between devices, body(): lax.psum_scatter(jnp.dot(dense_hidden, dense_down, preferred_element_type...  33.4 us
    all_gather x1, waiting for transfers between devices, body(): lax.all_gather(second, 'ep', axis=0, tiled=True)  32.8 us
    all_to_all x1, waiting for transfers between devices, body(): lax.all_to_all(answer.reshape(arrived_shape), 'ep', split_axis=1, concat_...  14.1 us
    unnamed x27, local copies, waits for them, and re-layouts  13 us
    all_to_all x1, starting transfers between devices, body(): lax.all_to_all(outgoing, 'ep', split_axis=0, concat_axis=1, tiled=True)  7.41 us
    dot_general x1, matrix products, body(): jnp.dot(dense_hidden, dense_down, preferred_element_type=jnp.float32)  4.14 us
    dot_general x2, matrix products, swiglu(): gate_part = jnp.dot(row_block, w_first, preferred_element_type=jnp.float32)  4.02 us
    all_to_all x1, starting transfers between devices, body(): lax.all_to_all(answer.reshape(arrived_shape), 'ep', split_axis=1, concat_...  3.68 us
  transfers between devices with their start and end apart: 4, of which 3 were waited for; matrix products, arithmetic and copies ran while one was open for 9% of the time, Pallas kernels for 0%

commit v1 on v0

--- a/solution.py
+++ b/solution.py
@@ -154,9 +154,11 @@
     answer = expert_rows(
         arrived.reshape(-1, arrived_shape[3]), expert_gate[0], expert_up[0], expert_down[0]
     )
-    returned = lax.all_to_all(
-        answer.reshape(arrived_shape), "ep", split_axis=1, concat_axis=0, tiled=True
-    )
+    fit_the_squares = lambda z_in, link_axis: jnp.concatenate(
+        lax.all_to_all(jnp.stack(jnp.split(z_in, lax.axis_size(link_axis), 1), 0), link_axis, 0, 0),
+        0,
+    )
+    returned = fit_the_squares(answer.reshape(arrived_shape), "ep")
     routed = jnp.dot(
         combine,
         returned.reshape(slot_total, -1).astype(jnp.float32),

time: 154 us -> 162 us (1.052)
  local copies, waits for them, and re-layouts: 13.8 us -> 23.5 us
    all_gather x1, waiting for transfers between devices: 32.8 us -> 14.2 us  [body(): lax.all_gather(second, 'ep', axis=0, tiled=True)]
    all_to_all x1, waiting for transfers between devices: 0.01 us -> 13.5 us  [body(): lax.all_to_all(outgoing, 'ep', split_axis=0, concat_axis=1, tiled=True)]
    unnamed x27 -> x44, local copies, waits for them, and re-layouts: 13 us -> 22.1 us
    reduce_scatter x1, waiting for transfers between devices: 33.4 us -> 37.5 us  [body(): lax.psum_scatter(jnp.dot(dense_hidden, dense_down, preferred_element_type...]
  transfers between devices with their start and end apart: 4 -> 4, of which waited for: 3 -> 4; matrix products, arithmetic and copies ran while one was open for 9% -> 9% of each run, Pallas kernels for 0% -> 0%
where the time goes in v1:
time: 162 us; the launch traced here: 161 us
  waiting for transfers between devices  80 us (49%)
  matrix products  28.6 us (18%)
  local copies, waits for them, and re-layouts  23.5 us (15%)
  between operations  13.6 us (8%)
  starting transfers between devices  11.2 us (7%)
  other arithmetic  3.86 us (2%)
    reduce_scatter x1, waiting for transfers between devices, body(): lax.psum_scatter(jnp.dot(dense_hidden, dense_down, preferred_element_type...  37.5 us
    unnamed x44, local copies, waits for them, and re-layouts  22.1 us
    all_gather x1, waiting for transfers between devices, body(): lax.all_gather(second, 'ep', axis=0, tiled=True)  14.2 us
    all_to_all x1, waiting for transfers between devices, body(): lax.all_to_all(jnp.stack(jnp.split(z_in, lax.axis_size(link_axis), 1), 0)...  14.1 us
    all_to_all x1, waiting for transfers between devices, body(): lax.all_to_all(outgoing, 'ep', split_axis=0, concat_axis=1, tiled=True)  13.5 us
    all_to_all x1, starting transfers between devices, body(): lax.all_to_all(outgoing, 'ep', split_axis=0, concat_axis=1, tiled=True)  7.41 us
    dot_general x2, matrix products, swiglu(): gate_part = jnp.dot(row_block, w_first, preferred_element_type=jnp.float32)  4.74 us
    dot_general x1, matrix products, body(): jnp.dot(dense_hidden, dense_down, preferred_element_type=jnp.float32)  4.18 us
  transfers between devices with their start and end apart: 4, of which 4 were waited for; matrix products, arithmetic and copies ran while one was open for 9% of the time, Pallas kernels for 0%

profile of v1, /device:TPU:0, one launch (start us, length us, event | category | flops | bytes accessed | tf_op | source)
XLA Modules:
  0.0 160.9 jit_solution(1650019868767233131)
XLA Ops:
  6.6 0.8 broadcast_add_fusion
  7.4 0.8 iota_compare_fusion
  8.2 1.0 fusion.43
  9.2 2.9 %convolution_convert_fusion.3 = bf16[16,1024]{1,0:T(8,128)(2,1)S(1)} fusion(bf16[2048,1024]{1,0:T(8,128)(2,1)} %param.24, bf16[16,2048]{1,0:T(8,128)(2,1)} %param.22, f32[2048]{0:T(1024)} %param.23, f32[16]{0:T(128)S(1)} %add_rsqrt_fusion.1), kind=kOutput, calls=%fused_computation.22 | convolution fusion | flops 67256320 | bytes 4300864 | tf_op jit(solution)/shard_map/dot_general | solution.py:45
  12.1 0.1 reshape.88
  12.3 0.2 fusion.46
  12.5 0.1 copy.52
  12.6 0.2 fusion.53
  12.8 0.1 copy.53
  12.9 0.1 broadcast_subtract_fusion
  13.0 6.5 %copy.51 = bf16[16,1024,128]{1,2,0:T(8,128)(2,1)} copy(bf16[16,1024,128]{2,1,0:T(8,128)(2,1)} %param.30) | data formatting | bytes 8388608 | tf_op args[8]
  19.5 0.2 convolution_convert_fusion.5
  19.7 0.1 reshape.101
  19.8 0.2 fusion.62
  20.0 3.0 %fusion.61 = (f32[16,2,8]{2,1,0:T(2,128)S(1)}, f32[16,2,8,1024]{3,2,1,0:T(8,128)S(1)}) fusion(f32[16,2,1024]{2,1,0:T(2,128)S(1)} %broadcast_subtract_fusion, bf16[16,2,8,64]{3,2,1,0:T(8,128)(2,1)S(1)} %reshape.88, bf16[16,1024,2,64]{1,3,2,0:T(8,128)(2,1)} %bitcast.132, pred[16,2,1024]{2,1,0:T(4,128)(4,1)S(1)} %iota_compare_fusion), kind=kOutput, calls=%fused_computation.117 | convolution fusion | flops 34602752 | bytes 5440512 | tf_op jit(solution)/shard_map/bgrd,blgd->bgrl/dot_general | solution.py:59
  22.9 0.3 fusion.24
  23.3 1.3 fusion.18
  24.6 0.1 reshape.95
  24.7 6.4 %copy.54 = bf16[16,1024,128]{1,2,0:T(8,128)(2,1)} copy(bf16[16,1024,128]{2,1,0:T(8,128)(2,1)} %param.31) | data formatting | bytes 8388608 | tf_op args[9]
  31.1 3.5 %fusion.17 = bf16[16,2,8,64]{3,2,1,0:T(8,128)(2,1)S(1)} fusion(bf16[16,1024,2,64]{1,3,2,0:T(8,128)(2,1)} %bitcast.133, f32[16,2,8,1024]{3,2,1,0:T(8,128)S(1)} %get-tuple-element.10, f32[16,2,8]{2,1,0:T(2,128)S(1)} %get-tuple-element.8, f32[16,2,8]{2,1,0:T(2,128)S(1)} %multiply_maximum_fusion, f32[16,2,64]{2,1,0:T(2,128)S(1)} %reshape.95, ...), kind=kOutput, calls=%fused_computation.21 | convolution fusion | flops 34390016 | bytes 5286912 | tf_op jit(solution)/shard_map/bgrl,blgd->bgrd/dot_general | solution.py:78
  34.6 0.1 convert_element_type.90
  34.7 3.0 %multiply_reduce_fusion = (f32[16]{0:T(128)S(1)}, f32[16,2048]{1,0:T(8,128)S(1)}) fusion(bf16[16,1024]{1,0:T(8,128)(2,1)S(1)} %convert_element_type.90, bf16[1024,2048]{1,0:T(8,128)(2,1)} %param.29, bf16[16,2048]{1,0:T(8,128)(2,1)S(1)} %copy-done.1), kind=kOutput, calls=%fused_computation.61 | convolution fusion | flops 67239920 | bytes 4423744 | tf_op jit(solution)/shard_map/dot_general | solution.py:125
  37.7 0.1 copy.55
  37.8 0.1 eq.31
  37.8 0.1 fusion.49
  37.9 0.1 reduce_window_sum.11
  38.0 0.2 select_reduce_fusion.1
  38.2 0.1 reduce_sum.70
  38.3 0.1 copy.56
  38.4 0.1 convert_reduce_fusion
  38.5 0.1 multiply_convert_fusion
  38.6 1.1 fusion
  39.7 7.4 %all-to-all-start = ((bf16[16,1,8,2048]{3,2,1,0:T(8,128)(2,1)}), bf16[16,1,8,2048]{3,2,1,0:T(8,128)(2,1)S(1)}, u32[]{:S(2)}, u32[]{:S(2)}) async-start(bf16[16,1,8,2048]{3,2,1,0:T(8,128)(2,1)} %fusion), calls=%async_computation.1 | async-start | bytes 1048576 | tf_op jit(solution)/shard_map/all_to_all | solution.py:152
  47.2 0.0 all-gather.2.cloned.1.call-start
  47.2 0.7 all-gather.2.cloned.1.call-update
  47.9 0.0 reduce-scatter.2.cloned.1.call-start
  47.9 13.5 %all-to-all-done = bf16[16,1,8,2048]{3,2,1,0:T(8,128)(2,1)S(1)} async-done(((bf16[16,1,8,2048]{3,2,1,0:T(8,128)(2,1)}), bf16[16,1,8,2048]{3,2,1,0:T(8,128)(2,1)S(1)}, u32[]{:S(2)}, u32[]{:S(2)}) %all-to-all-start) | async-done | bytes 524320 | tf_op jit(solution)/shard_map/all_to_all | solution.py:152
  61.4 2.8 %fusion.6 = f32[128,512]{1,0:T(8,128)} fusion(bf16[1,2048,512]{2,1,0:T(8,128)(2,1)} %param.39, bf16[16,1,8,2048]{3,2,1,0:T(8,128)(2,1)S(1)} %all-to-all-done), kind=kOutput, calls=%fused_computation.11 | convolution fusion | flops 268435456 | bytes 2883584 | tf_op jit(solution)/shard_map/dot_general | solution.py:17
  64.2 2.4 %fusion.1 = bf16[1,16,8,2048]{3,2,1,0:T(8,128)(2,1)S(1)} fusion(bf16[1,512,2048]{2,1,0:T(8,128)(2,1)S(1)} %copy-done, bf16[1,2048,512]{2,1,0:T(8,128)(2,1)} %param.40, bf16[16,1,8,2048]{3,2,1,0:T(8,128)(2,1)S(1)} %all-to-all-done, f32[128,512]{1,0:T(8,128)} %fusion.6), kind=kOutput, calls=%fused_computation.4 | convolution fusion | flops 537526272 | bytes 5505024 | tf_op jit(solution)/shard_map/dot_general | solution.py:24
  66.6 0.6 constant_dynamic-update-slice_fusion.15
  67.2 0.6 constant_dynamic-update-slice_fusion.14
  67.8 0.6 constant_dynamic-update-slice_fusion.13
  68.5 0.6 constant_dynamic-update-slice_fusion.12
  69.1 0.6 constant_dynamic-update-slice_fusion.11
  69.7 0.6 constant_dynamic-update-slice_fusion.10
  70.3 0.6 constant_dynamic-update-slice_fusion.9
  70.9 0.6 constant_dynamic-update-slice_fusion.8
  71.5 0.6 constant_dynamic-update-slice_fusion.7
  72.1 0.6 constant_dynamic-update-slice_fusion.6
  72.7 0.6 constant_dynamic-update-slice_fusion.5
  73.3 0.6 constant_dynamic-update-slice_fusion.4
  73.9 0.6 constant_dynamic-update-slice_fusion.3
  74.5 0.6 constant_dynamic-update-slice_fusion.2
  75.1 14.2 %all-gather.2.cloned.1.call-done = bf16[256,2048]{1,0:T(8,128)(2,1)} async-done(((bf16[16,2048]{1,0:T(8,128)(2,1)}), bf16[256,2048]{1,0:T(8,128)(2,1)}) %all-gather.2.cloned.1.call-update) | async-done | bytes 1048592 | tf_op jit(solution)/shard_map/all_gather | solution.py:167
  89.4 2.0 %fusion.63 = f32[256,256]{1,0:T(8,128)S(1)} fusion(bf16[256,2048]{1,0:T(8,128)(2,1)} %all-gather.2.cloned.1.call-done, bf16[2048,256]{1,0:T(8,128)(2,1)} %param.36), kind=kOutput, calls=%fused_computation.119 | convolution fusion | flops 268435456 | bytes 2359296 | tf_op jit(solution)/shard_map/dot_general | solution.py:17
  91.3 4.2 %convolution_convert_fusion = bf16[256,2048]{1,0:T(8,128)(2,1)} fusion(bf16[256,2048]{1,0:T(8,128)(2,1)} %param.38, bf16[256,2048]{1,0:T(8,128)(2,1)} %all-gather.2.cloned.1.call-done, bf16[2048,256]{1,0:T(8,128)(2,1)} %param.37, f32[256,256]{1,0:T(8,128)S(1)} %fusion.63), kind=kOutput, calls=%fused_computation | convolution fusion | flops 537788416 | bytes 4456448 | tf_op jit(solution)/shard_map/dot_general | solution.py:169
  95.5 0.0 reduce-scatter.2.cloned.1.call-update
  95.5 0.6 constant_dynamic-update-slice_fusion.1
  96.1 0.6 constant_dynamic-update-slice_fusion
  96.7 3.7 %all-to-all-start.1 = ((bf16[16,1,1,8,2048]{4,3,2,1,0:T(8,128)(2,1)}), bf16[16,1,1,8,2048]{4,3,2,1,0:T(8,128)(2,1)S(1)}, u32[]{:S(2)}, u32[]{:S(2)}) async-start(bf16[16,1,1,8,2048]{4,3,2,1,0:T(8,128)(2,1)} %constant_dynamic-update-slice_fusion), calls=%async_computation.2 | async-start | bytes 1048576 | tf_op jit(solution)/shard_map/all_to_all | solution.py:158
  100.5 0.1 fusion.23
  100.6 14.1 %all-to-all-done.1 = bf16[16,1,1,8,2048]{4,3,2,1,0:T(8,128)(2,1)S(1)} async-done(((bf16[16,1,1,8,2048]{4,3,2,1,0:T(8,128)(2,1)}), bf16[16,1,1,8,2048]{4,3,2,1,0:T(8,128)(2,1)S(1)}, u32[]{:S(2)}, u32[]{:S(2)}) %all-to-all-start.1) | async-done | bytes 524320 | tf_op jit(solution)/shard_map/all_to_all | solution.py:158
  114.7 37.5 %reduce-scatter.2.cloned.1.call-done = bf16[16,2048]{1,0:T(8,128)(2,1)} async-done(((bf16[256,2048]{1,0:T(8,128)(2,1)}), bf16[16,2048]{1,0:T(8,128)(2,1)}) %reduce-scatter.2.cloned.1.call-update) | async-done | bytes 65552 | tf_op jit(solution)/shard_map/reduce_scatter | solution.py:168
  152.2 1.8 %fusion.2 = bf16[16,2048]{1,0:T(8,128)(2,1)} fusion(f32[128,16]{0,1:T(8,128)S(1)} %get-tuple-element.6, bf16[16,1,1,8,2048]{4,3,2,1,0:T(8,128)(2,1)S(1)} %all-to-all-done.1, f32[16,2048]{1,0:T(8,128)S(1)} %get-tuple-element.12, bf16[16,2048]{1,0:T(8,128)(2,1)} %reduce-scatter.2.cloned.1.call-done, f32[16]{0:T(128)S(1)} %fusion.23), kind=kOutput, calls=%fused_computation.7 | convolution fusion | flops 50495488 | bytes 794688 | tf_op jit(solution)/shard_map/dot_general | solution.py:162
  (31 shorter events, 0.1 us)
Async XLA Ops:
  6.5 57.7 %copy-start = (bf16[1,512,2048]{2,1,0:T(8,128)(2,1)S(1)}, bf16[1,512,2048]{2,1,0:T(8,128)(2,1)}, u32[]{:S(2)}) copy-start(bf16[1,512,2048]{2,1,0:T(8,128)(2,1)} %param.41) | copy-start | bytes 6291460
  6.5 6.0 %copy-start.1 = (bf16[16,2048]{1,0:T(8,128)(2,1)S(1)}, bf16[16,2048]{1,0:T(8,128)(2,1)}, u32[]{:S(2)}) copy-start(bf16[16,2048]{1,0:T(8,128)(2,1)} %param.22) | copy-start | bytes 196612
  6.5 6.0 %copy-start.6 = (f32[2048]{0:T(1024)S(1)}, f32[2048]{0:T(1024)}, u32[]{:S(2)}) copy-start(f32[2048]{0:T(1024)} %param.23) | copy-start | bytes 24580
  6.5 5.7 %copy-start.5 = (f32[16,2,1024]{2,1,0:T(2,128)S(1)}, f32[16,2,1024]{2,1,0:T(2,128)}, u32[]{:S(2)}) copy-start(f32[16,2,1024]{2,1,0:T(2,128)} %param.32) | copy-start | bytes 393220
  6.5 6.0 %copy-start.10 = (bf16[2048,2]{0,1:T(2,128)(2,1)S(1)}, bf16[2048,2]{0,1:T(2,128)(2,1)}, u32[]{:S(2)}) copy-start(bf16[2048,2]{0,1:T(2,128)(2,1)} %param.27) | copy-start | bytes 24580
  6.5 6.0 %copy-start.12 = (f32[2]{0:T(128)S(1)}, f32[2]{0:T(128)}, u32[]{:S(2)}) copy-start(f32[2]{0:T(128)} %param.28) | copy-start | bytes 28
  13.0 6.5 %copy-start.4 = (bf16[2048,128]{1,0:T(8,128)(2,1)S(1)}, bf16[2048,128]{1,0:T(8,128)(2,1)}, u32[]{:S(2)}) copy-start(bf16[2048,128]{1,0:T(8,128)(2,1)} %param.25) | copy-start | bytes 1572868
  31.1 6.6 %copy-start.8 = (s32[16,4]{0,1:T(4,128)S(1)}, s32[16,4]{0,1:T(4,128)}, u32[]{:S(2)}) copy-start(s32[16,4]{0,1:T(4,128)} %param.42) | copy-start | bytes 772
  31.1 7.3 %copy-start.9 = (f32[16,4]{0,1:T(4,128)S(1)}, f32[16,4]{0,1:T(4,128)}, u32[]{:S(2)}) copy-start(f32[16,4]{0,1:T(4,128)} %param.43) | copy-start | bytes 772
  31.1 7.4 %copy-start.7 = (f32[2048]{0:T(1024)S(1)}, f32[2048]{0:T(1024)}, u32[]{:S(2)}) copy-start(f32[2048]{0:T(1024)} %param.34) | copy-start | bytes 24580
  38.6 8.6 %copy-start.2 = (bf16[16,2048]{1,0:T(8,128)(2,1)}, bf16[16,2048]{1,0:T(8,128)(2,1)S(1)}, u32[]{:S(2)}) copy-start(bf16[16,2048]{1,0:T(8,128)(2,1)S(1)} %multiply_convert_fusion) | copy-start | bytes 196612
  39.7 21.7 %all-to-all-start = ((bf16[16,1,8,2048]{3,2,1,0:T(8,128)(2,1)}), bf16[16,1,8,2048]{3,2,1,0:T(8,128)(2,1)S(1)}, u32[]{:S(2)}, u32[]{:S(2)}) async-start(bf16[16,1,8,2048]{3,2,1,0:T(8,128)(2,1)} %fusion), calls=%async_computation.1 | async-start | bytes 1048576 | tf_op jit(solution)/shard_map/all_to_all | solution.py:152
  47.2 42.2 %all-gather.2.cloned.1.call-start = ((), (), s32[]{:S(2)}) async-start(), calls=%async_computation.3 | async-start | bytes 1114112 | tf_op jit(solution)/shard_map/all_gather | solution.py:167
  47.9 104.3 %reduce-scatter.2.cloned.1.call-start = ((), (), s32[]{:S(2)}) async-start(), calls=%async_computation.4 | async-start | bytes 1114112 | tf_op jit(solution)/shard_map/reduce_scatter | solution.py:168
  75.1 25.3 %copy-start.3 = (bf16[16,2048]{1,0:T(8,128)(2,1)S(1)}, bf16[16,2048]{1,0:T(8,128)(2,1)}, u32[]{:S(2)}) copy-start(bf16[16,2048]{1,0:T(8,128)(2,1)} %copy-done.2) | copy-start | bytes 196612
  75.1 25.3 %copy-start.11 = (f32[2048]{0:T(1024)S(1)}, f32[2048]{0:T(1024)}, u32[]{:S(2)}) copy-start(f32[2048]{0:T(1024)} %param.35) | copy-start | bytes 24580
  96.7 18.0 %all-to-all-start.1 = ((bf16[16,1,1,8,2048]{4,3,2,1,0:T(8,128)(2,1)}), bf16[16,1,1,8,2048]{4,3,2,1,0:T(8,128)(2,1)S(1)}, u32[]{:S(2)}, u32[]{:S(2)}) async-start(bf16[16,1,1,8,2048]{4,3,2,1,0:T(8,128)(2,1)} %constant_dynamic-update-slice_fusion), calls=%async_computation.2 | async-start | bytes 1048576 | tf_op jit(solution)/shard_map/all_to_all | solution.py:158
Sparse Core Ops, SparseCore 0:
  50.1 39.1 all-gather.1
  95.7 56.5 reduce-scatter.1
